TPU v7x, 32 devices: a whole 2x2x4 slice. The times are simulated.
32 devices in a mesh: grp: 2 (over y), sp: 4 (over z), tp: 4 (over x, core).
Axes of the slice: x: 2, y: 2, z: 4, core: 2. Of those that a mesh axis runs over, the one named last changes fastest.
Arguments:
- queries: bfloat16 [1024, 2048], P(('grp', 'sp'), 'tp'), parts along dimension 0, may hold values from -8 to 8
- keys: bfloat16 [1024, 1024], P(('grp', 'sp'), 'tp'), parts along dimension 0, may hold values from -6 to 6
- values: bfloat16 [1024, 1024], P(('grp', 'sp'), 'tp'), parts along dimension 0, may hold values from -6 to 6
- head_bias: float32 [16], P('tp'), may hold values from -15 to -5
- documents: int32 [1024], P(('grp', 'sp')), parts along dimension 0, may hold values from 0 to 2, never falling along the last dimension, each value on 1 to 384 neighbouring positions
- w_out: bfloat16 [2048, 2048], P('tp'), may hold values from -0.125 to 0.125
- resid: bfloat16 [1024, 2048], P(('grp', 'sp', 'tp')), parts along dimension 0, may hold values from -6 to 6
- norm_gain: float32 [2048], replicated, may hold values from 0.1 to 1.9
- expert_ids: int32 [1024, 2], P(('grp', 'sp', 'tp')), parts along dimension 0, may hold values from 0 to 3, all different within a row; in each aligned block of 32 rows (0 to 31, 32 to 63, ...) at most 32 rows name the same one
- expert_gates: float32 [1024, 2], P(('grp', 'sp', 'tp')), parts along dimension 0, may hold values from 0.1 to 0.9
- w_gate: bfloat16 [4, 2048, 3072], P('sp', None, 'tp'), may hold values from -0.125 to 0.125
- w_up: bfloat16 [4, 2048, 3072], P('sp', None, 'tp'), may hold values from -0.125 to 0.125
- w_down: bfloat16 [4, 3072, 2048], P('sp', 'tp'), may hold values from -0.109375 to 0.109375
Outputs:
- layer_out: bfloat16 [1024, 2048], P(('grp', 'sp', 'tp')), parts along dimension 0
There are 2 independent parts, one for each index of `grp`. A program takes and returns all parts, laid end to end along the dimension named above; an argument that names none is the same for every part. Nothing has to cross between parts.
Inputs may be any that keep to these rules, and one draw needn't show every extreme that they name: Document numbers never fall along the sequence; each of the 3 documents holds at least one position and the longest exactly 384 positions. `expert_ids`: each position names 2 different experts. Among the 32 positions of one device (aligned blocks of 32 rows) no expert is named more than 32 times, and in some block some expert exactly 32 times.
All inputs are finite; a program needn't handle non-finite values.
Results may differ from a plain program's by a relative error of at most 0.012.
Values may be sent and summed in bfloat16 or wider, within the bound.
No kernel may reach another device: no remote copies, remote signals or barrier semaphores. Data moves between devices by JAX's collectives and lax.ppermute only.
A program may use at most 64 MiB of HBM per device.

v0:
```python
import jax
import jax.numpy as jnp
from jax import lax
from jax.sharding import PartitionSpec as P

D = 2048
HEADS = 16
KV_HEADS = 8
DH = 128
TOPK = 2


def passed_along(value, axis, steps):
    count = lax.axis_size(axis)
    initial, last = (max(0, -steps), min(count, count - steps))
    return lax.ppermute(value, axis, [(source, source + steps) for source in range(initial, last)])


def attend_terms(query_grid, bias_grid, key_block, value_block, live, carried):
    kv_local = bias_grid.shape[0]
    key_count = key_block.shape[0]
    logits = (
        jnp.einsum(
            "qgrd,sgd->grqs",
            query_grid,
            key_block.reshape(key_count, kv_local, DH),
            preferred_element_type=jnp.float32,
        )
        * DH ** (-0.5)
        + bias_grid[:, :, None, None]
    )
    keep = jnp.where(live, jax.nn.log_sigmoid(-logits), 0.0)
    after = lax.cumsum(keep, axis=3, reverse=True) - keep + carried[:, :, :, None]
    weight = jnp.where(live, jnp.exp(jax.nn.log_sigmoid(logits) + after), 0.0).astype(jnp.bfloat16)
    partial_mix = jnp.einsum(
        "grqs,sgd->qgrd",
        weight,
        value_block.reshape(key_count, kv_local, DH),
        preferred_element_type=jnp.float32,
    )
    return (partial_mix, jnp.sum(keep, axis=3))


def local(
    queries,
    keys,
    values,
    head_bias,
    documents,
    w_out,
    resid,
    norm_gain,
    expert_ids,
    expert_gates,
    w_gate,
    w_up,
    w_down,
):
    tok_count = queries.shape[0]
    kv_local = keys.shape[1] // DH
    group_size = HEADS // KV_HEADS
    sp_count = lax.axis_size("sp")
    tp_count = lax.axis_size("tp")
    sp_index = lax.axis_index("sp")
    query_grid = queries.reshape(tok_count, kv_local, group_size, DH)
    bias_grid = head_bias.reshape(kv_local, group_size)
    doc_here = documents.astype(jnp.bfloat16)
    doc_column = doc_here.reshape(tok_count, 1)
    local_pos = jnp.arange(tok_count, dtype=jnp.int32)
    live_local = (local_pos[None, :] < local_pos[:, None]) & (
        documents[None, :] == documents[:, None]
    )
    zero_carry = jnp.zeros((kv_local, group_size, tok_count), jnp.float32)
    mix_total, carried = attend_terms(query_grid, bias_grid, keys, values, live_local, zero_carry)

    def visit(turn_index, state):
        mix_sum, carry_sum, key_block, value_block, doc_block = state
        key_block, value_block, doc_block = passed_along(
            (key_block, value_block, doc_block), "sp", 1
        )
        live = (doc_block[:, 0][None, :] == doc_here[:, None]) & (sp_index - turn_index >= 0)
        partial_mix, block_keep = attend_terms(
            query_grid, bias_grid, key_block, value_block, live, carry_sum
        )
        return (mix_sum + partial_mix, carry_sum + block_keep, key_block, value_block, doc_block)

    mix_total, carried, key_last, value_last, doc_last = lax.fori_loop(
        1, sp_count, visit, (mix_total, carried, keys, values, doc_column)
    )
    mixed = mix_total.reshape(tok_count, kv_local * group_size * DH).astype(jnp.bfloat16)
    projected = lax.psum_scatter(
        jnp.dot(mixed, w_out, preferred_element_type=jnp.float32).astype(jnp.bfloat16),
        "tp",
        scatter_dimension=0,
        tiled=True,
    ).astype(jnp.float32)
    middle = (resid.astype(jnp.float32) + projected).astype(jnp.bfloat16)
    middle_value = middle.astype(jnp.float32)
    normed = (
        middle_value
        * lax.rsqrt(jnp.mean(middle_value * middle_value, axis=1, keepdims=True) + 1e-06)
        * norm_gain
    ).astype(jnp.bfloat16)
    row_count = normed.shape[0]
    expert_count = w_gate.shape[0] * sp_count
    slot_limit = min(row_count, max(2, 2 * TOPK * row_count // expert_count))
    flat_ids = expert_ids.reshape(-1)
    onehot_ids = (flat_ids[:, None] == jnp.arange(expert_count, dtype=jnp.int32)[None, :]).astype(
        jnp.int32
    )
    earlier = jnp.cumsum(onehot_ids, axis=0) - onehot_ids
    slot_ids = jnp.sum(earlier * onehot_ids, axis=1)
    target = flat_ids * slot_limit + slot_ids
    placing = (
        jnp.arange(expert_count * slot_limit, dtype=jnp.int32)[:, None] == target[None, :]
    ).astype(jnp.bfloat16)
    by_token = jnp.sum(placing.reshape(expert_count * slot_limit, row_count, TOPK), axis=2)
    outgoing = jnp.dot(by_token, normed, preferred_element_type=jnp.float32).astype(jnp.bfloat16)
    outgoing = outgoing.reshape(expert_count, slot_limit, D)
    arrived = lax.all_to_all(outgoing, "sp", split_axis=0, concat_axis=0, tiled=True)
    gathered = lax.all_gather(arrived, "tp", axis=0, tiled=True)
    expert_rows = gathered.reshape(-1, D)
    gate_value = jnp.dot(expert_rows, w_gate[0], preferred_element_type=jnp.float32)
    up_value = jnp.dot(expert_rows, w_up[0], preferred_element_type=jnp.float32)
    hidden = (jax.nn.silu(gate_value) * up_value).astype(jnp.bfloat16)
    partial_out = jnp.dot(hidden, w_down[0], preferred_element_type=jnp.float32)
    summed = lax.psum_scatter(
        partial_out.reshape(tp_count, sp_count * slot_limit, D).astype(jnp.bfloat16),
        "tp",
        scatter_dimension=0,
        tiled=True,
    ).astype(jnp.float32)
    expert_result = summed.reshape(sp_count, slot_limit, D).astype(jnp.bfloat16)
    returned = lax.all_to_all(expert_result, "sp", split_axis=0, concat_axis=0, tiled=True)
    routed = jnp.dot(placing.T, returned.reshape(-1, D), preferred_element_type=jnp.float32)
    combined = jnp.sum(expert_gates[:, :, None] * routed.reshape(row_count, TOPK, D), axis=1)
    return (middle_value + combined).astype(jnp.bfloat16)


def solution(mesh):
    return jax.shard_map(
        local,
        mesh=mesh,
        in_specs=(
            P(("grp", "sp"), "tp"),
            P(("grp", "sp"), "tp"),
            P(("grp", "sp"), "tp"),
            P("tp"),
            P(("grp", "sp")),
            P("tp", None),
            P(("grp", "sp", "tp"), None),
            P(),
            P(("grp", "sp", "tp"), None),
            P(("grp", "sp", "tp"), None),
            P("sp", None, "tp"),
            P("sp", None, "tp"),
            P("sp", "tp", None),
        ),
        out_specs=P(("grp", "sp", "tp"), None),
        check_vma=False,
    )
```

profile of v0, /device:TPU:0, one launch (start us, length us, event | category | flops | bytes accessed | tf_op | source)
XLA Modules:
  0.0 232.2 jit_solution(13194715823110891600)
XLA Ops:
  17.9 2.4 %fusion.56 = (f32[2,2,128]{2,1,0:T(2,128)}, f32[2,2,128,128]{2,3,1,0:T(8,128)S(1)}, f32[2,2,128,128]{2,3,1,0:T(8,128)}) fusion(pred[128,128]{0,1:T(8,128)(4,1)S(1)} %fusion.50, f32[2,2]{1,0:T(2,128)} %add.157, bf16[128,2,2,128]{0,3,2,1:T(8,128)(2,1)S(1)} %bitcast.78, bf16[128,2,128,1]{2,1,0,3:T(2,128)(2,1)} %bitcast.81), kind=kOutput, calls=%fused_computation.74 | convolution fusion | flops 17497600 | bytes 739344 | tf_op jit(solution)/shard_map/qgrd,sgd->grqs/dot_general | solution.py:23
  20.3 5.1 %reduce_window_sum.31 = f32[2,2,128,128]{2,3,1,0:T(8,128)} reduce-window(f32[2,2,128,128]{2,3,1,0:T(8,128)S(1)} %get-tuple-element.239, f32[]{:T(128)} %constant.57.clone.1), window={size=1x1x1x128 pad=0_0x0_0x0_0x0_127}, to_apply=%region_0.1 | reduce-window | flops 8323072 | bytes 524292 | tf_op jit(solution)/shard_map/attend_terms/reduce_window_sum | solution.py:33
  27.7 69.8 %while.21 = (s32[]{:T(128)}, f32[128,2,2,128]{3,0,2,1:T(8,128)}, f32[2,2,128]{2,1,0:T(2,128)}, bf16[128,256]{0,1:T(8,128)(2,1)}, bf16[128,256]{0,1:T(8,128)(2,1)...) while((s32[]{:T(128)}, f32[128,2,2,128]{3,0,2,1:T(8,128)}, ...), condition=%wide.region_5.6_spmd, body=%wide.region_2.5_spmd.sunk | while | flops 44105732 | bytes 3207487 | solution.py:87
  27.7 4.9 %collective-permute-start.1 = (bf16[128,1]{0,1:T(2,128)(2,1)}, bf16[128,1]{0,1:T(2,128)(2,1)S(1)}, u32[]{:S(2)}, u32[]{:S(2)}) collective-permute-start(bf16[128,1]{0,1:T(2,128)(2,1)} %get-tuple-element.328), channel_id=1, source_target_pairs={{0,4},{4,8},{8,12},{1,5},{5,9},{9,13},{2,6},{6,10},{10,14},{3,7},{... | collective-permute-start | bytes 776 | tf_op jit(solution)/shard_map/while/body/eval_jaxpr/ppermute | solution.py:16
  32.7 3.5 %collective-permute-start.2 = (bf16[128,256]{0,1:T(8,128)(2,1)}, bf16[128,256]{0,1:T(8,128)(2,1)S(1)}, u32[]{:S(2)}, u32[]{:S(2)}) collective-permute-start(bf16[128,256]{0,1:T(8,128)(2,1)} %get-tuple-element.326), channel_id=1, source_target_pairs={{0,4},{4,8},{8,12},{1,5},{5,9},{9,13},{2,6},{6,10},{10,14},{3,7},{... | collective-permute-start | bytes 196616 | tf_op jit(solution)/shard_map/while/body/eval_jaxpr/ppermute | solution.py:16
  36.2 3.5 %collective-permute-start = (bf16[128,256]{0,1:T(8,128)(2,1)}, bf16[128,256]{0,1:T(8,128)(2,1)S(1)}, u32[]{:S(2)}, u32[]{:S(2)}) collective-permute-start(bf16[128,256]{0,1:T(8,128)(2,1)} %get-tuple-element.327), channel_id=1, source_target_pairs={{0,4},{4,8},{8,12},{1,5},{5,9},{9,13},{2,6},{6,10},{10,14},{3,7},{... | collective-permute-start | bytes 196616 | tf_op jit(solution)/shard_map/while/body/eval_jaxpr/ppermute | solution.py:16
  41.7 2.6 %fusion.80 = (f32[2,2,128]{2,1,0:T(2,128)}, f32[2,2,128,128]{2,3,1,0:T(8,128)}, f32[2,2,128,128]{2,3,1,0:T(8,128)}) fusion(pred[128,128]{0,1:T(8,128)(4,1)S(1)} %compare_and_fusion.2, f32[2,2]{1,0:T(2,128)S(1)} %add.252, bf16[128,2,128,1]{0,2,3,1:T(8,128)(2,1)S(1)} %bitcast.74, bf16[128,2,2,128]{3,0,2,1:T(8,128)(2,1)} %get-tuple-element.344), kind=kOutput, calls=%fused_computation.19.clone.1 | convolution fusion | flops 17497600 | bytes 739344 | tf_op jit(solution)/shard_map/while/body/eval_jaxpr/qgrd,sgd->grqs/dot_general | solution.py:23
  44.3 5.4 %reduce_window_sum.34 = f32[2,2,128,128]{2,3,1,0:T(8,128)S(1)} reduce-window(f32[2,2,128,128]{2,3,1,0:T(8,128)} %get-tuple-element.307, f32[]{:T(128)} %constant.57.clone.1..sunk), window={size=1x1x1x128 pad=0_0x0_0x0_0x0_127}, to_apply=%region_3.3 | reduce-window | flops 8323072 | bytes 524292 | tf_op jit(solution)/shard_map/while/body/eval_jaxpr/reduce_window_sum | solution.py:33
  56.4 2.6 %collective-permute-start.2 = (bf16[128,256]{0,1:T(8,128)(2,1)}, bf16[128,256]{0,1:T(8,128)(2,1)S(1)}, u32[]{:S(2)}, u32[]{:S(2)}) collective-permute-start(bf16[128,256]{0,1:T(8,128)(2,1)} %get-tuple-element.326), channel_id=1, source_target_pairs={{0,4},{4,8},{8,12},{1,5},{5,9},{9,13},{2,6},{6,10},{10,14},{3,7},{... | collective-permute-start | bytes 196616 | tf_op jit(solution)/shard_map/while/body/eval_jaxpr/ppermute | solution.py:16
  63.0 2.6 %fusion.80 = (f32[2,2,128]{2,1,0:T(2,128)}, f32[2,2,128,128]{2,3,1,0:T(8,128)}, f32[2,2,128,128]{2,3,1,0:T(8,128)}) fusion(pred[128,128]{0,1:T(8,128)(4,1)S(1)} %compare_and_fusion.2, f32[2,2]{1,0:T(2,128)S(1)} %add.252, bf16[128,2,128,1]{0,2,3,1:T(8,128)(2,1)S(1)} %bitcast.74, bf16[128,2,2,128]{3,0,2,1:T(8,128)(2,1)} %get-tuple-element.344), kind=kOutput, calls=%fused_computation.19.clone.1 | convolution fusion | flops 17497600 | bytes 739344 | tf_op jit(solution)/shard_map/while/body/eval_jaxpr/qgrd,sgd->grqs/dot_general | solution.py:23
  65.6 5.4 %reduce_window_sum.34 = f32[2,2,128,128]{2,3,1,0:T(8,128)S(1)} reduce-window(f32[2,2,128,128]{2,3,1,0:T(8,128)} %get-tuple-element.307, f32[]{:T(128)} %constant.57.clone.1..sunk), window={size=1x1x1x128 pad=0_0x0_0x0_0x0_127}, to_apply=%region_3.3 | reduce-window | flops 8323072 | bytes 524292 | tf_op jit(solution)/shard_map/while/body/eval_jaxpr/reduce_window_sum | solution.py:33
  71.0 2.3 fusion.81
  75.8 2.7 %collective-permute-start.1 = (bf16[128,1]{0,1:T(2,128)(2,1)}, bf16[128,1]{0,1:T(2,128)(2,1)S(1)}, u32[]{:S(2)}, u32[]{:S(2)}) collective-permute-start(bf16[128,1]{0,1:T(2,128)(2,1)} %get-tuple-element.328), channel_id=1, source_target_pairs={{0,4},{4,8},{8,12},{1,5},{5,9},{9,13},{2,6},{6,10},{10,14},{3,7},{... | collective-permute-start | bytes 776 | tf_op jit(solution)/shard_map/while/body/eval_jaxpr/ppermute | solution.py:16
  84.7 2.6 %fusion.80 = (f32[2,2,128]{2,1,0:T(2,128)}, f32[2,2,128,128]{2,3,1,0:T(8,128)}, f32[2,2,128,128]{2,3,1,0:T(8,128)}) fusion(pred[128,128]{0,1:T(8,128)(4,1)S(1)} %compare_and_fusion.2, f32[2,2]{1,0:T(2,128)S(1)} %add.252, bf16[128,2,128,1]{0,2,3,1:T(8,128)(2,1)S(1)} %bitcast.74, bf16[128,2,2,128]{3,0,2,1:T(8,128)(2,1)} %get-tuple-element.344), kind=kOutput, calls=%fused_computation.19.clone.1 | convolution fusion | flops 17497600 | bytes 739344 | tf_op jit(solution)/shard_map/while/body/eval_jaxpr/qgrd,sgd->grqs/dot_general | solution.py:23
  87.3 5.4 %reduce_window_sum.34 = f32[2,2,128,128]{2,3,1,0:T(8,128)S(1)} reduce-window(f32[2,2,128,128]{2,3,1,0:T(8,128)} %get-tuple-element.307, f32[]{:T(128)} %constant.57.clone.1..sunk), window={size=1x1x1x128 pad=0_0x0_0x0_0x0_127}, to_apply=%region_3.3 | reduce-window | flops 8323072 | bytes 524292 | tf_op jit(solution)/shard_map/while/body/eval_jaxpr/reduce_window_sum | solution.py:33
  98.6 2.9 %convolution_convert_fusion.1 = bf16[128,2048]{1,0:T(8,128)(2,1)} fusion(bf16[128,512]{0,1:T(8,128)(2,1)S(1)} %bitcast.79, bf16[512,2048]{1,0:T(8,128)(2,1)} %param.20), kind=kOutput, calls=%fused_computation.28 | convolution fusion | flops 268697600 | bytes 2752512 | tf_op jit(solution)/shard_map/dot_general | solution.py:92
  102.6 19.0 %reduce-scatter.3.cloned.1.call-done = bf16[32,2048]{1,0:T(8,128)(2,1)} async-done(((bf16[128,2048]{1,0:T(8,128)(2,1)}), bf16[32,2048]{1,0:T(8,128)(2,1)}) %reduce-scatter.3.cloned.1.call-update) | async-done | bytes 131088 | tf_op jit(solution)/shard_map/reduce_scatter | solution.py:91
  123.9 18.8 %all_to_all.10 = bf16[4,32,2048]{2,1,0:T(8,128)(2,1)} all-to-all(bf16[4,32,2048]{2,1,0:T(8,128)(2,1)S(1)} %bitcast.73), channel_id=1, replica_groups=mesh['grp'=2,'sp'=4,'tp'=4] {'sp'}, dimensions={0} | all-to-all | bytes 1048576 | tf_op jit(solution)/shard_map/all_to_all | solution.py:120
  142.8 20.8 %all-gather.2.cloned.1.call-done = bf16[16,32,2048]{2,1,0:T(8,128)(2,1)} async-done(((bf16[4,32,2048]{2,1,0:T(8,128)(2,1)}), bf16[16,32,2048]{2,1,0:T(8,128)(2,1)}) %all-gather.2.cloned.1.call-update) | async-done | bytes 2097168 | tf_op jit(solution)/shard_map/all_gather | solution.py:121
  163.6 4.5 %fusion.21 = f32[512,768]{1,0:T(8,128)S(1)} fusion(bf16[512,2048]{1,0:T(8,128)(2,1)} %bitcast.83, bf16[1,2048,768]{2,1,0:T(8,128)(2,1)} %param.25), kind=kOutput, calls=%fused_computation.24 | convolution fusion | flops 1610612736 | bytes 6815744 | tf_op jit(solution)/shard_map/dot_general | solution.py:123
  170.0 3.2 %fusion.23 = bf16[4,128,2048]{2,1,0:T(8,128)(2,1)} fusion(bf16[4,128,768]{2,1,0:T(8,128)(2,1)S(1)} %bitcast.85, bf16[1,768,2048]{2,1,0:T(8,128)(2,1)S(1)} %copy-done), kind=kOutput, calls=%fused_computation.26 | convolution fusion | flops 1611661312 | bytes 6029312 | tf_op jit(solution)/shard_map/dot_general | solution.py:126
  173.3 31.3 %reduce-scatter.5.cloned.1.call-done = bf16[1,128,2048]{2,1,0:T(8,128)(2,1)} async-done(((bf16[4,128,2048]{2,1,0:T(8,128)(2,1)}), bf16[1,128,2048]{2,1,0:T(8,128)(2,1)}) %reduce-scatter.5.cloned.1.call-update) | async-done | bytes 524304 | tf_op jit(solution)/shard_map/reduce_scatter | solution.py:127
  204.6 4.6 %all-to-all-start.1 = ((bf16[4,32,2048]{2,1,0:T(8,128)(2,1)}), bf16[4,32,2048]{2,1,0:T(8,128)(2,1)}, u32[]{:S(2)}, u32[]{:S(2)}) async-start(bf16[4,32,2048]{2,1,0:T(8,128)(2,1)} %bitcast.76), calls=%async_computation.3 | async-start | bytes 1048576 | tf_op jit(solution)/shard_map/all_to_all | solution.py:134
  209.3 14.3 %all-to-all-done.1 = bf16[4,32,2048]{2,1,0:T(8,128)(2,1)} async-done(((bf16[4,32,2048]{2,1,0:T(8,128)(2,1)}), bf16[4,32,2048]{2,1,0:T(8,128)(2,1)}, u32[]{:S(2)}, u32[]{:S(2)}) %all-to-all-start.1) | async-done | bytes 524320 | tf_op jit(solution)/shard_map/all_to_all | solution.py:134
  (84 shorter events, 48.3 us)
Async XLA Ops:
  6.5 163.5 %copy-start = (bf16[1,768,2048]{2,1,0:T(8,128)(2,1)S(1)}, bf16[1,768,2048]{2,1,0:T(8,128)(2,1)}, u32[]{:S(2)}) copy-start(bf16[1,768,2048]{2,1,0:T(8,128)(2,1)} %param.27) | copy-start | bytes 9437188
  6.5 115.0 %reduce-scatter.3.cloned.1.call-start = ((), (), s32[]{:S(2)}) async-start(), calls=%async_computation.4 | async-start | bytes 655360 | tf_op jit(solution)/shard_map/reduce_scatter | solution.py:91
  27.7 12.7 %collective-permute-start.1 = (bf16[128,1]{0,1:T(2,128)(2,1)}, bf16[128,1]{0,1:T(2,128)(2,1)S(1)}, u32[]{:S(2)}, u32[]{:S(2)}) collective-permute-start(bf16[128,1]{0,1:T(2,128)(2,1)} %get-tuple-element.328), channel_id=1, source_target_pairs={{0,4},{4,8},{8,12},{1,5},{5,9},{9,13},{2,6},{6,10},{10,14},{3,7},{... | collective-permute-start | bytes 776 | tf_op jit(solution)/shard_map/while/body/eval_jaxpr/ppermute | solution.py:16
  32.7 9.0 %collective-permute-start.2 = (bf16[128,256]{0,1:T(8,128)(2,1)}, bf16[128,256]{0,1:T(8,128)(2,1)S(1)}, u32[]{:S(2)}, u32[]{:S(2)}) collective-permute-start(bf16[128,256]{0,1:T(8,128)(2,1)} %get-tuple-element.326), channel_id=1, source_target_pairs={{0,4},{4,8},{8,12},{1,5},{5,9},{9,13},{2,6},{6,10},{10,14},{3,7},{... | collective-permute-start | bytes 196616 | tf_op jit(solution)/shard_map/while/body/eval_jaxpr/ppermute | solution.py:16
  36.2 13.5 %collective-permute-start = (bf16[128,256]{0,1:T(8,128)(2,1)}, bf16[128,256]{0,1:T(8,128)(2,1)S(1)}, u32[]{:S(2)}, u32[]{:S(2)}) collective-permute-start(bf16[128,256]{0,1:T(8,128)(2,1)} %get-tuple-element.327), channel_id=1, source_target_pairs={{0,4},{4,8},{8,12},{1,5},{5,9},{9,13},{2,6},{6,10},{10,14},{3,7},{... | collective-permute-start | bytes 196616 | tf_op jit(solution)/shard_map/while/body/eval_jaxpr/ppermute | solution.py:16
  54.5 7.2 %collective-permute-start.1 = (bf16[128,1]{0,1:T(2,128)(2,1)}, bf16[128,1]{0,1:T(2,128)(2,1)S(1)}, u32[]{:S(2)}, u32[]{:S(2)}) collective-permute-start(bf16[128,1]{0,1:T(2,128)(2,1)} %get-tuple-element.328), channel_id=1, source_target_pairs={{0,4},{4,8},{8,12},{1,5},{5,9},{9,13},{2,6},{6,10},{10,14},{3,7},{... | collective-permute-start | bytes 776 | tf_op jit(solution)/shard_map/while/body/eval_jaxpr/ppermute | solution.py:16
  56.4 6.6 %collective-permute-start.2 = (bf16[128,256]{0,1:T(8,128)(2,1)}, bf16[128,256]{0,1:T(8,128)(2,1)S(1)}, u32[]{:S(2)}, u32[]{:S(2)}) collective-permute-start(bf16[128,256]{0,1:T(8,128)(2,1)} %get-tuple-element.326), channel_id=1, source_target_pairs={{0,4},{4,8},{8,12},{1,5},{5,9},{9,13},{2,6},{6,10},{10,14},{3,7},{... | collective-permute-start | bytes 196616 | tf_op jit(solution)/shard_map/while/body/eval_jaxpr/ppermute | solution.py:16
  59.0 12.0 %collective-permute-start = (bf16[128,256]{0,1:T(8,128)(2,1)}, bf16[128,256]{0,1:T(8,128)(2,1)S(1)}, u32[]{:S(2)}, u32[]{:S(2)}) collective-permute-start(bf16[128,256]{0,1:T(8,128)(2,1)} %get-tuple-element.327), channel_id=1, source_target_pairs={{0,4},{4,8},{8,12},{1,5},{5,9},{9,13},{2,6},{6,10},{10,14},{3,7},{... | collective-permute-start | bytes 196616 | tf_op jit(solution)/shard_map/while/body/eval_jaxpr/ppermute | solution.py:16
  75.8 7.6 %collective-permute-start.1 = (bf16[128,1]{0,1:T(2,128)(2,1)}, bf16[128,1]{0,1:T(2,128)(2,1)S(1)}, u32[]{:S(2)}, u32[]{:S(2)}) collective-permute-start(bf16[128,1]{0,1:T(2,128)(2,1)} %get-tuple-element.328), channel_id=1, source_target_pairs={{0,4},{4,8},{8,12},{1,5},{5,9},{9,13},{2,6},{6,10},{10,14},{3,7},{... | collective-permute-start | bytes 776 | tf_op jit(solution)/shard_map/while/body/eval_jaxpr/ppermute | solution.py:16
  78.5 6.2 %collective-permute-start.2 = (bf16[128,256]{0,1:T(8,128)(2,1)}, bf16[128,256]{0,1:T(8,128)(2,1)S(1)}, u32[]{:S(2)}, u32[]{:S(2)}) collective-permute-start(bf16[128,256]{0,1:T(8,128)(2,1)} %get-tuple-element.326), channel_id=1, source_target_pairs={{0,4},{4,8},{8,12},{1,5},{5,9},{9,13},{2,6},{6,10},{10,14},{3,7},{... | collective-permute-start | bytes 196616 | tf_op jit(solution)/shard_map/while/body/eval_jaxpr/ppermute | solution.py:16
  80.7 12.0 %collective-permute-start = (bf16[128,256]{0,1:T(8,128)(2,1)}, bf16[128,256]{0,1:T(8,128)(2,1)S(1)}, u32[]{:S(2)}, u32[]{:S(2)}) collective-permute-start(bf16[128,256]{0,1:T(8,128)(2,1)} %get-tuple-element.327), channel_id=1, source_target_pairs={{0,4},{4,8},{8,12},{1,5},{5,9},{9,13},{2,6},{6,10},{10,14},{3,7},{... | collective-permute-start | bytes 196616 | tf_op jit(solution)/shard_map/while/body/eval_jaxpr/ppermute | solution.py:16
  97.5 4.2 %copy-start.4 = (s32[32,2]{0,1:T(2,128)S(1)}, s32[32,2]{0,1:T(2,128)}, u32[]{:S(2)}) copy-start(s32[32,2]{0,1:T(2,128)} %param.23) | copy-start | bytes 772
  97.5 24.1 %copy-start.1 = (bf16[32,2048]{1,0:T(8,128)(2,1)S(1)}, bf16[32,2048]{1,0:T(8,128)(2,1)}, u32[]{:S(2)}) copy-start(bf16[32,2048]{1,0:T(8,128)(2,1)} %param.21) | copy-start | bytes 393220
  97.5 25.1 %copy-start.3 = (f32[2048]{0:T(1024)S(1)}, f32[2048]{0:T(1024)}, u32[]{:S(2)}) copy-start(f32[2048]{0:T(1024)} %param.22) | copy-start | bytes 24580
  101.5 62.1 %all-gather.2.cloned.1.call-start = ((), (), s32[]{:S(2)}) async-start(), calls=%async_computation.5 | async-start | bytes 2621440 | tf_op jit(solution)/shard_map/all_gather | solution.py:121
  142.8 61.8 %reduce-scatter.5.cloned.1.call-start = ((), (), s32[]{:S(2)}) async-start(), calls=%async_computation.6 | async-start | bytes 2621440 | tf_op jit(solution)/shard_map/reduce_scatter | solution.py:127
  163.6 4.5 %copy-start.6 = (bf16[1,2048,768]{2,1,0:T(8,128)(2,1)S(1)}, bf16[1,2048,768]{2,1,0:T(8,128)(2,1)}, u32[]{:S(2)}) copy-start(bf16[1,2048,768]{2,1,0:T(8,128)(2,1)} %param.26) | copy-start | bytes 9437188
  163.6 4.5 %copy-start.7 = (bf16[16,32,2048]{2,1,0:T(8,128)(2,1)S(1)}, bf16[16,32,2048]{2,1,0:T(8,128)(2,1)}, u32[]{:S(2)}) copy-start(bf16[16,32,2048]{2,1,0:T(8,128)(2,1)} %all-gather.2.cloned.1.call-done) | copy-start | bytes 6291460
  173.2 50.4 %copy-start.5 = (f32[32,2]{0,1:T(2,128)S(1)}, f32[32,2]{0,1:T(2,128)}, u32[]{:S(2)}) copy-start(f32[32,2]{0,1:T(2,128)} %param.24) | copy-start | bytes 772
  173.2 51.7 %copy-start.2 = (bf16[32,2048]{1,0:T(8,128)(2,1)S(1)}, bf16[32,2048]{1,0:T(8,128)(2,1)}, u32[]{:S(2)}) copy-start(bf16[32,2048]{1,0:T(8,128)(2,1)} %reduce-scatter.3.cloned.1.call-done) | copy-start | bytes 393220
  204.6 19.1 %all-to-all-start.1 = ((bf16[4,32,2048]{2,1,0:T(8,128)(2,1)}), bf16[4,32,2048]{2,1,0:T(8,128)(2,1)}, u32[]{:S(2)}, u32[]{:S(2)}) async-start(bf16[4,32,2048]{2,1,0:T(8,128)(2,1)} %bitcast.76), calls=%async_computation.3 | async-start | bytes 1048576 | tf_op jit(solution)/shard_map/all_to_all | solution.py:134
Sparse Core Ops, SparseCore 0:
  101.7 19.8 reduce-scatter.2
  142.9 20.6 all-gather.1
  173.4 31.1 reduce-scatter.4
where the time goes:
time: 233 us; the launch traced here: 232 us
  waiting for transfers between devices  85.5 us (37%)
  matrix products  34.5 us (15%)
  other arithmetic  31.5 us (14%)
  starting transfers between devices  30.1 us (13%)
  blocking collectives  18.8 us (8%)
  local copies, waits for them, and re-layouts  18.3 us (8%)
  between operations  13.2 us (6%)
    reduce_scatter x1, waiting for transfers between devices, local(): lax.psum_scatter(partial_out.reshape(tp_count, sp_count * slot_limit, D)....  31.3 us
    ppermute x9, starting transfers between devices, passed_along(): lax.ppermute(value, axis, [(source, source + steps) for source in range(i...  25.2 us
    another operation x4, other arithmetic, attend_terms(): lax.cumsum(keep, axis=3, reverse=True) - keep + carried[:, :, :, None]  21.2 us
    all_gather x1, waiting for transfers between devices, local(): gathered = lax.all_gather(arrived, 'tp', axis=0, tiled=True)  20.8 us
    reduce_scatter x1, waiting for transfers between devices, local(): lax.psum_scatter(jnp.dot(mixed, w_out, preferred_element_type=jnp.float32...  19 us
    all_to_all x1, blocking collectives, local(): lax.all_to_all(outgoing, 'sp', split_axis=0, concat_axis=0, tiled=True)  18.8 us
    all_to_all x1, waiting for transfers between devices, local(): lax.all_to_all(expert_result, 'sp', split_axis=0, concat_axis=0, tiled=True)  14.3 us
    dot_general x4, matrix products, attend_terms(): jnp.einsum('qgrd,sgd->grqs', query_grid, key_block.reshape(key_count, kv_...  10.4 us
  transfers between devices with their start and end apart: 13, of which 4 were waited for; matrix products, arithmetic and copies ran while one was open for 13% of the time, Pallas kernels for 0%

commit v1 on v0

--- a/solution.py
+++ b/solution.py
@@ -118,7 +118,20 @@
     outgoing = jnp.dot(by_token, normed, preferred_element_type=jnp.float32).astype(jnp.bfloat16)
     outgoing = outgoing.reshape(expert_count, slot_limit, D)
     arrived = lax.all_to_all(outgoing, "sp", split_axis=0, concat_axis=0, tiled=True)
-    gathered = lax.all_gather(arrived, "tp", axis=0, tiled=True)
+
+    def connect_point(m):
+        all_blocks = [m]
+        degree = lax.psum(1, axis_name="tp")
+        for pp in range(degree - 1):
+            piece_out = lax.ppermute(
+                all_blocks[-1], axis_name="tp", perm=[(s, (s + 1) % degree) for s in range(degree)]
+            )
+            all_blocks.append(piece_out)
+        passed = jnp.concatenate(all_blocks[::-1], 0)
+        b_next = lax.axis_index("tp")
+        return jnp.roll(passed, (b_next + 1) * m.shape[0], axis=0)
+
+    gathered = connect_point(arrived)
     expert_rows = gathered.reshape(-1, D)
     gate_value = jnp.dot(expert_rows, w_gate[0], preferred_element_type=jnp.float32)
     up_value = jnp.dot(expert_rows, w_up[0], preferred_element_type=jnp.float32)

time: 233 us -> 244 us (1.047)
  local copies, waits for them, and re-layouts: 18.3 us -> 27.3 us
  waiting for transfers between devices: 85.5 us -> 89.1 us
  matrix products: 34.5 us -> 31.8 us
    ppermute x0 -> x3, waiting for transfers between devices: none -> 26.2 us  [connect_point(): lax.ppermute(all_blocks[-1], axis_name='tp', perm=[(s, (s + 1) % degree)...]
    all_gather x1 -> x0, waiting for transfers between devices: 20.8 us -> none  [local(): gathered = lax.all_gather(arrived, 'tp', axis=0, tiled=True)]
    unnamed x18 -> x33, local copies, waits for them, and re-layouts: 1.14 us -> 9.82 us
    dot_general x1, matrix products: 4.45 us -> 1.81 us  [local(): jnp.dot(expert_rows, w_gate[0], preferred_element_type=jnp.float32)]
  transfers between devices with their start and end apart: 13 -> 15, of which waited for: 4 -> 6; matrix products, arithmetic and copies ran while one was open for 13% -> 13% of each run, Pallas kernels for 0% -> 0%
where the time goes in v1:
time: 244 us; the launch traced here: 242 us
  waiting for transfers between devices  89.1 us (37%)
  matrix products  31.8 us (13%)
  other arithmetic  31.5 us (13%)
  starting transfers between devices  30.1 us (12%)
  local copies, waits for them, and re-layouts  27.3 us (11%)
  blocking collectives  18.7 us (8%)
  between operations  13.6 us (6%)
    reduce_scatter x1, waiting for transfers between devices, local(): lax.psum_scatter(partial_out.reshape(tp_count, sp_count * slot_limit, D)....  29.5 us
    ppermute x3, waiting for transfers between devices, connect_point(): lax.ppermute(all_blocks[-1], axis_name='tp', perm=[(s, (s + 1) % degree)...  26.2 us
    ppermute x9, starting transfers between devices, passed_along(): lax.ppermute(value, axis, [(source, source + steps) for source in range(i...  25.2 us
    another operation x4, other arithmetic, attend_terms(): lax.cumsum(keep, axis=3, reverse=True) - keep + carried[:, :, :, None]  21.2 us
    reduce_scatter x1, waiting for transfers between devices, local(): lax.psum_scatter(jnp.dot(mixed, w_out, preferred_element_type=jnp.float32...  19 us
    all_to_all x1, blocking collectives, local(): lax.all_to_all(outgoing, 'sp', split_axis=0, concat_axis=0, tiled=True)  18.7 us
    all_to_all x1, waiting for transfers between devices, local(): lax.all_to_all(expert_result, 'sp', split_axis=0, concat_axis=0, tiled=True)  14.3 us
    dot_general x4, matrix products, attend_terms(): jnp.einsum('qgrd,sgd->grqs', query_grid, key_block.reshape(key_count, kv_...  10.4 us
  transfers between devices with their start and end apart: 15, of which 6 were waited for; matrix products, arithmetic and copies ran while one was open for 13% of the time, Pallas kernels for 0%

profile of v1, /device:TPU:0, one launch (start us, length us, event | category | flops | bytes accessed | tf_op | source)
XLA Modules:
  0.0 242.2 jit_solution(18398306935887122782)
XLA Ops:
  17.9 2.4 %fusion.56 = (f32[2,2,128]{2,1,0:T(2,128)}, f32[2,2,128,128]{2,3,1,0:T(8,128)S(1)}, f32[2,2,128,128]{2,3,1,0:T(8,128)}) fusion(pred[128,128]{0,1:T(8,128)(4,1)S(1)} %fusion.50, f32[2,2]{1,0:T(2,128)} %add.170, bf16[128,2,2,128]{0,3,2,1:T(8,128)(2,1)S(1)} %bitcast.80, bf16[128,2,128,1]{2,1,0,3:T(2,128)(2,1)} %bitcast.83), kind=kOutput, calls=%fused_computation.83 | convolution fusion | flops 17497600 | bytes 739344 | tf_op jit(solution)/shard_map/qgrd,sgd->grqs/dot_general | solution.py:23
  20.3 5.1 %reduce_window_sum.31 = f32[2,2,128,128]{2,3,1,0:T(8,128)} reduce-window(f32[2,2,128,128]{2,3,1,0:T(8,128)S(1)} %get-tuple-element.229, f32[]{:T(128)} %constant.78.clone.1), window={size=1x1x1x128 pad=0_0x0_0x0_0x0_127}, to_apply=%region_0.1 | reduce-window | flops 8323072 | bytes 524292 | tf_op jit(solution)/shard_map/attend_terms/reduce_window_sum | solution.py:33
  27.7 69.8 %while.21 = (s32[]{:T(128)}, f32[128,2,2,128]{3,0,2,1:T(8,128)}, f32[2,2,128]{2,1,0:T(2,128)}, bf16[128,256]{0,1:T(8,128)(2,1)}, bf16[128,256]{0,1:T(8,128)(2,1)...) while((s32[]{:T(128)}, f32[128,2,2,128]{3,0,2,1:T(8,128)}, ...), condition=%wide.region_5.6_spmd, body=%wide.region_2.5_spmd.sunk | while | flops 44105732 | bytes 3207487 | solution.py:87
  27.7 4.9 %collective-permute-start.1 = (bf16[128,1]{0,1:T(2,128)(2,1)}, bf16[128,1]{0,1:T(2,128)(2,1)S(1)}, u32[]{:S(2)}, u32[]{:S(2)}) collective-permute-start(bf16[128,1]{0,1:T(2,128)(2,1)} %get-tuple-element.318), channel_id=1, source_target_pairs={{0,4},{4,8},{8,12},{1,5},{5,9},{9,13},{2,6},{6,10},{10,14},{3,7},{... | collective-permute-start | bytes 776 | tf_op jit(solution)/shard_map/while/body/eval_jaxpr/ppermute | solution.py:16
  32.7 3.5 %collective-permute-start.2 = (bf16[128,256]{0,1:T(8,128)(2,1)}, bf16[128,256]{0,1:T(8,128)(2,1)S(1)}, u32[]{:S(2)}, u32[]{:S(2)}) collective-permute-start(bf16[128,256]{0,1:T(8,128)(2,1)} %get-tuple-element.316), channel_id=1, source_target_pairs={{0,4},{4,8},{8,12},{1,5},{5,9},{9,13},{2,6},{6,10},{10,14},{3,7},{... | collective-permute-start | bytes 196616 | tf_op jit(solution)/shard_map/while/body/eval_jaxpr/ppermute | solution.py:16
  36.2 3.5 %collective-permute-start = (bf16[128,256]{0,1:T(8,128)(2,1)}, bf16[128,256]{0,1:T(8,128)(2,1)S(1)}, u32[]{:S(2)}, u32[]{:S(2)}) collective-permute-start(bf16[128,256]{0,1:T(8,128)(2,1)} %get-tuple-element.317), channel_id=1, source_target_pairs={{0,4},{4,8},{8,12},{1,5},{5,9},{9,13},{2,6},{6,10},{10,14},{3,7},{... | collective-permute-start | bytes 196616 | tf_op jit(solution)/shard_map/while/body/eval_jaxpr/ppermute | solution.py:16
  41.7 2.6 %fusion.80 = (f32[2,2,128]{2,1,0:T(2,128)}, f32[2,2,128,128]{2,3,1,0:T(8,128)}, f32[2,2,128,128]{2,3,1,0:T(8,128)}) fusion(pred[128,128]{0,1:T(8,128)(4,1)S(1)} %compare_and_fusion.2, f32[2,2]{1,0:T(2,128)S(1)} %add.268, bf16[128,2,128,1]{0,2,3,1:T(8,128)(2,1)S(1)} %bitcast.76, bf16[128,2,2,128]{3,0,2,1:T(8,128)(2,1)} %get-tuple-element.334), kind=kOutput, calls=%fused_computation.19.clone.1 | convolution fusion | flops 17497600 | bytes 739344 | tf_op jit(solution)/shard_map/while/body/eval_jaxpr/qgrd,sgd->grqs/dot_general | solution.py:23
  44.3 5.4 %reduce_window_sum.34 = f32[2,2,128,128]{2,3,1,0:T(8,128)S(1)} reduce-window(f32[2,2,128,128]{2,3,1,0:T(8,128)} %get-tuple-element.297, f32[]{:T(128)} %constant.78.clone.1..sunk), window={size=1x1x1x128 pad=0_0x0_0x0_0x0_127}, to_apply=%region_3.3 | reduce-window | flops 8323072 | bytes 524292 | tf_op jit(solution)/shard_map/while/body/eval_jaxpr/reduce_window_sum | solution.py:33
  56.4 2.6 %collective-permute-start.2 = (bf16[128,256]{0,1:T(8,128)(2,1)}, bf16[128,256]{0,1:T(8,128)(2,1)S(1)}, u32[]{:S(2)}, u32[]{:S(2)}) collective-permute-start(bf16[128,256]{0,1:T(8,128)(2,1)} %get-tuple-element.316), channel_id=1, source_target_pairs={{0,4},{4,8},{8,12},{1,5},{5,9},{9,13},{2,6},{6,10},{10,14},{3,7},{... | collective-permute-start | bytes 196616 | tf_op jit(solution)/shard_map/while/body/eval_jaxpr/ppermute | solution.py:16
  63.0 2.6 %fusion.80 = (f32[2,2,128]{2,1,0:T(2,128)}, f32[2,2,128,128]{2,3,1,0:T(8,128)}, f32[2,2,128,128]{2,3,1,0:T(8,128)}) fusion(pred[128,128]{0,1:T(8,128)(4,1)S(1)} %compare_and_fusion.2, f32[2,2]{1,0:T(2,128)S(1)} %add.268, bf16[128,2,128,1]{0,2,3,1:T(8,128)(2,1)S(1)} %bitcast.76, bf16[128,2,2,128]{3,0,2,1:T(8,128)(2,1)} %get-tuple-element.334), kind=kOutput, calls=%fused_computation.19.clone.1 | convolution fusion | flops 17497600 | bytes 739344 | tf_op jit(solution)/shard_map/while/body/eval_jaxpr/qgrd,sgd->grqs/dot_general | solution.py:23
  65.6 5.4 %reduce_window_sum.34 = f32[2,2,128,128]{2,3,1,0:T(8,128)S(1)} reduce-window(f32[2,2,128,128]{2,3,1,0:T(8,128)} %get-tuple-element.297, f32[]{:T(128)} %constant.78.clone.1..sunk), window={size=1x1x1x128 pad=0_0x0_0x0_0x0_127}, to_apply=%region_3.3 | reduce-window | flops 8323072 | bytes 524292 | tf_op jit(solution)/shard_map/while/body/eval_jaxpr/reduce_window_sum | solution.py:33
  75.8 2.6 %collective-permute-start.1 = (bf16[128,1]{0,1:T(2,128)(2,1)}, bf16[128,1]{0,1:T(2,128)(2,1)S(1)}, u32[]{:S(2)}, u32[]{:S(2)}) collective-permute-start(bf16[128,1]{0,1:T(2,128)(2,1)} %get-tuple-element.318), channel_id=1, source_target_pairs={{0,4},{4,8},{8,12},{1,5},{5,9},{9,13},{2,6},{6,10},{10,14},{3,7},{... | collective-permute-start | bytes 776 | tf_op jit(solution)/shard_map/while/body/eval_jaxpr/ppermute | solution.py:16
  84.7 2.6 %fusion.80 = (f32[2,2,128]{2,1,0:T(2,128)}, f32[2,2,128,128]{2,3,1,0:T(8,128)}, f32[2,2,128,128]{2,3,1,0:T(8,128)}) fusion(pred[128,128]{0,1:T(8,128)(4,1)S(1)} %compare_and_fusion.2, f32[2,2]{1,0:T(2,128)S(1)} %add.268, bf16[128,2,128,1]{0,2,3,1:T(8,128)(2,1)S(1)} %bitcast.76, bf16[128,2,2,128]{3,0,2,1:T(8,128)(2,1)} %get-tuple-element.334), kind=kOutput, calls=%fused_computation.19.clone.1 | convolution fusion | flops 17497600 | bytes 739344 | tf_op jit(solution)/shard_map/while/body/eval_jaxpr/qgrd,sgd->grqs/dot_general | solution.py:23
  87.4 5.4 %reduce_window_sum.34 = f32[2,2,128,128]{2,3,1,0:T(8,128)S(1)} reduce-window(f32[2,2,128,128]{2,3,1,0:T(8,128)} %get-tuple-element.297, f32[]{:T(128)} %constant.78.clone.1..sunk), window={size=1x1x1x128 pad=0_0x0_0x0_0x0_127}, to_apply=%region_3.3 | reduce-window | flops 8323072 | bytes 524292 | tf_op jit(solution)/shard_map/while/body/eval_jaxpr/reduce_window_sum | solution.py:33
  98.7 2.9 %convolution_convert_fusion.1 = bf16[128,2048]{1,0:T(8,128)(2,1)} fusion(bf16[128,512]{0,1:T(8,128)(2,1)S(1)} %bitcast.81, bf16[512,2048]{1,0:T(8,128)(2,1)} %param.20), kind=kOutput, calls=%fused_computation.28 | convolution fusion | flops 268697600 | bytes 2752512 | tf_op jit(solution)/shard_map/dot_general | solution.py:92
  102.6 19.0 %reduce-scatter.3.cloned.1.call-done = bf16[32,2048]{1,0:T(8,128)(2,1)} async-done(((bf16[128,2048]{1,0:T(8,128)(2,1)}), bf16[32,2048]{1,0:T(8,128)(2,1)}) %reduce-scatter.3.cloned.1.call-update) | async-done | bytes 131088 | tf_op jit(solution)/shard_map/reduce_scatter | solution.py:91
  123.9 18.7 %all_to_all.10 = bf16[4,32,2048]{2,1,0:T(8,128)(2,1)S(1)} all-to-all(bf16[4,32,2048]{2,1,0:T(8,128)(2,1)S(1)} %bitcast.75), channel_id=1, replica_groups=mesh['grp'=2,'sp'=4,'tp'=4] {'sp'}, dimensions={0} | all-to-all | bytes 1048576 | tf_op jit(solution)/shard_map/all_to_all | solution.py:120
  143.5 8.6 %collective-permute-done.3 = bf16[4,32,2048]{2,1,0:T(8,128)(2,1)S(1)} collective-permute-done((bf16[4,32,2048]{2,1,0:T(8,128)(2,1)S(1)}, bf16[4,32,2048]{2,1,0:T(8,128)(2,1)S(1)}, u32[]{:S(2)}, u32[]{:S(2)}) %collective-permute-start.3) | collective-permute-done | bytes 524320 | tf_op jit(solution)/shard_map/ppermute | solution.py:126
  152.9 8.7 %collective-permute-done.4 = bf16[4,32,2048]{2,1,0:T(8,128)(2,1)} collective-permute-done((bf16[4,32,2048]{2,1,0:T(8,128)(2,1)S(1)}, bf16[4,32,2048]{2,1,0:T(8,128)(2,1)}, u32[]{:S(2)}, u32[]{:S(2)}) %collective-permute-start.4) | collective-permute-done | bytes 524320 | tf_op jit(solution)/shard_map/ppermute | solution.py:126
  161.6 8.9 %collective-permute-done.5 = bf16[4,32,2048]{2,1,0:T(8,128)(2,1)} collective-permute-done((bf16[4,32,2048]{2,1,0:T(8,128)(2,1)}, bf16[4,32,2048]{2,1,0:T(8,128)(2,1)}, u32[]{:S(2)}, u32[]{:S(2)}) %collective-permute-start.5) | collective-permute-done | bytes 524320 | tf_op jit(solution)/shard_map/ppermute | solution.py:126
  181.7 3.2 %fusion.23 = bf16[4,128,2048]{2,1,0:T(8,128)(2,1)} fusion(bf16[4,128,768]{2,1,0:T(8,128)(2,1)S(1)} %bitcast.85, bf16[1,768,2048]{2,1,0:T(8,128)(2,1)S(1)} %copy-done), kind=kOutput, calls=%fused_computation.26 | convolution fusion | flops 1611661312 | bytes 6029312 | tf_op jit(solution)/shard_map/dot_general | solution.py:139
  184.9 29.5 %reduce-scatter.5.cloned.1.call-done = bf16[1,128,2048]{2,1,0:T(8,128)(2,1)} async-done(((bf16[4,128,2048]{2,1,0:T(8,128)(2,1)}), bf16[1,128,2048]{2,1,0:T(8,128)(2,1)}) %reduce-scatter.5.cloned.1.call-update) | async-done | bytes 524304 | tf_op jit(solution)/shard_map/reduce_scatter | solution.py:140
  214.4 4.6 %all-to-all-start.1 = ((bf16[4,32,2048]{2,1,0:T(8,128)(2,1)}), bf16[4,32,2048]{2,1,0:T(8,128)(2,1)}, u32[]{:S(2)}, u32[]{:S(2)}) async-start(bf16[4,32,2048]{2,1,0:T(8,128)(2,1)} %bitcast.78), calls=%async_computation.3 | async-start | bytes 1048576 | tf_op jit(solution)/shard_map/all_to_all | solution.py:147
  219.1 14.3 %all-to-all-done.1 = bf16[4,32,2048]{2,1,0:T(8,128)(2,1)} async-done(((bf16[4,32,2048]{2,1,0:T(8,128)(2,1)}), bf16[4,32,2048]{2,1,0:T(8,128)(2,1)}, u32[]{:S(2)}, u32[]{:S(2)}) %all-to-all-start.1) | async-done | bytes 524320 | tf_op jit(solution)/shard_map/all_to_all | solution.py:147
  (104 shorter events, 61.3 us)
Async XLA Ops:
  6.5 175.1 %copy-start = (bf16[1,768,2048]{2,1,0:T(8,128)(2,1)S(1)}, bf16[1,768,2048]{2,1,0:T(8,128)(2,1)}, u32[]{:S(2)}) copy-start(bf16[1,768,2048]{2,1,0:T(8,128)(2,1)} %param.27) | copy-start | bytes 9437188
  6.5 115.0 %reduce-scatter.3.cloned.1.call-start = ((), (), s32[]{:S(2)}) async-start(), calls=%async_computation.4 | async-start | bytes 655360 | tf_op jit(solution)/shard_map/reduce_scatter | solution.py:91
  27.7 12.7 %collective-permute-start.1 = (bf16[128,1]{0,1:T(2,128)(2,1)}, bf16[128,1]{0,1:T(2,128)(2,1)S(1)}, u32[]{:S(2)}, u32[]{:S(2)}) collective-permute-start(bf16[128,1]{0,1:T(2,128)(2,1)} %get-tuple-element.318), channel_id=1, source_target_pairs={{0,4},{4,8},{8,12},{1,5},{5,9},{9,13},{2,6},{6,10},{10,14},{3,7},{... | collective-permute-start | bytes 776 | tf_op jit(solution)/shard_map/while/body/eval_jaxpr/ppermute | solution.py:16
  32.7 9.0 %collective-permute-start.2 = (bf16[128,256]{0,1:T(8,128)(2,1)}, bf16[128,256]{0,1:T(8,128)(2,1)S(1)}, u32[]{:S(2)}, u32[]{:S(2)}) collective-permute-start(bf16[128,256]{0,1:T(8,128)(2,1)} %get-tuple-element.316), channel_id=1, source_target_pairs={{0,4},{4,8},{8,12},{1,5},{5,9},{9,13},{2,6},{6,10},{10,14},{3,7},{... | collective-permute-start | bytes 196616 | tf_op jit(solution)/shard_map/while/body/eval_jaxpr/ppermute | solution.py:16
  36.2 13.5 %collective-permute-start = (bf16[128,256]{0,1:T(8,128)(2,1)}, bf16[128,256]{0,1:T(8,128)(2,1)S(1)}, u32[]{:S(2)}, u32[]{:S(2)}) collective-permute-start(bf16[128,256]{0,1:T(8,128)(2,1)} %get-tuple-element.317), channel_id=1, source_target_pairs={{0,4},{4,8},{8,12},{1,5},{5,9},{9,13},{2,6},{6,10},{10,14},{3,7},{... | collective-permute-start | bytes 196616 | tf_op jit(solution)/shard_map/while/body/eval_jaxpr/ppermute | solution.py:16
  54.5 7.2 %collective-permute-start.1 = (bf16[128,1]{0,1:T(2,128)(2,1)}, bf16[128,1]{0,1:T(2,128)(2,1)S(1)}, u32[]{:S(2)}, u32[]{:S(2)}) collective-permute-start(bf16[128,1]{0,1:T(2,128)(2,1)} %get-tuple-element.318), channel_id=1, source_target_pairs={{0,4},{4,8},{8,12},{1,5},{5,9},{9,13},{2,6},{6,10},{10,14},{3,7},{... | collective-permute-start | bytes 776 | tf_op jit(solution)/shard_map/while/body/eval_jaxpr/ppermute | solution.py:16
  56.4 6.6 %collective-permute-start.2 = (bf16[128,256]{0,1:T(8,128)(2,1)}, bf16[128,256]{0,1:T(8,128)(2,1)S(1)}, u32[]{:S(2)}, u32[]{:S(2)}) collective-permute-start(bf16[128,256]{0,1:T(8,128)(2,1)} %get-tuple-element.316), channel_id=1, source_target_pairs={{0,4},{4,8},{8,12},{1,5},{5,9},{9,13},{2,6},{6,10},{10,14},{3,7},{... | collective-permute-start | bytes 196616 | tf_op jit(solution)/shard_map/while/body/eval_jaxpr/ppermute | solution.py:16
  59.1 12.0 %collective-permute-start = (bf16[128,256]{0,1:T(8,128)(2,1)}, bf16[128,256]{0,1:T(8,128)(2,1)S(1)}, u32[]{:S(2)}, u32[]{:S(2)}) collective-permute-start(bf16[128,256]{0,1:T(8,128)(2,1)} %get-tuple-element.317), channel_id=1, source_target_pairs={{0,4},{4,8},{8,12},{1,5},{5,9},{9,13},{2,6},{6,10},{10,14},{3,7},{... | collective-permute-start | bytes 196616 | tf_op jit(solution)/shard_map/while/body/eval_jaxpr/ppermute | solution.py:16
  75.8 7.6 %collective-permute-start.1 = (bf16[128,1]{0,1:T(2,128)(2,1)}, bf16[128,1]{0,1:T(2,128)(2,1)S(1)}, u32[]{:S(2)}, u32[]{:S(2)}) collective-permute-start(bf16[128,1]{0,1:T(2,128)(2,1)} %get-tuple-element.318), channel_id=1, source_target_pairs={{0,4},{4,8},{8,12},{1,5},{5,9},{9,13},{2,6},{6,10},{10,14},{3,7},{... | collective-permute-start | bytes 776 | tf_op jit(solution)/shard_map/while/body/eval_jaxpr/ppermute | solution.py:16
  78.5 6.2 %collective-permute-start.2 = (bf16[128,256]{0,1:T(8,128)(2,1)}, bf16[128,256]{0,1:T(8,128)(2,1)S(1)}, u32[]{:S(2)}, u32[]{:S(2)}) collective-permute-start(bf16[128,256]{0,1:T(8,128)(2,1)} %get-tuple-element.316), channel_id=1, source_target_pairs={{0,4},{4,8},{8,12},{1,5},{5,9},{9,13},{2,6},{6,10},{10,14},{3,7},{... | collective-permute-start | bytes 196616 | tf_op jit(solution)/shard_map/while/body/eval_jaxpr/ppermute | solution.py:16
  80.7 12.1 %collective-permute-start = (bf16[128,256]{0,1:T(8,128)(2,1)}, bf16[128,256]{0,1:T(8,128)(2,1)S(1)}, u32[]{:S(2)}, u32[]{:S(2)}) collective-permute-start(bf16[128,256]{0,1:T(8,128)(2,1)} %get-tuple-element.317), channel_id=1, source_target_pairs={{0,4},{4,8},{8,12},{1,5},{5,9},{9,13},{2,6},{6,10},{10,14},{3,7},{... | collective-permute-start | bytes 196616 | tf_op jit(solution)/shard_map/while/body/eval_jaxpr/ppermute | solution.py:16
  97.5 4.2 %copy-start.8 = (s32[32,2]{0,1:T(2,128)S(1)}, s32[32,2]{0,1:T(2,128)}, u32[]{:S(2)}) copy-start(s32[32,2]{0,1:T(2,128)} %param.23) | copy-start | bytes 772
  97.5 24.0 %copy-start.5 = (bf16[32,2048]{1,0:T(8,128)(2,1)S(1)}, bf16[32,2048]{1,0:T(8,128)(2,1)}, u32[]{:S(2)}) copy-start(bf16[32,2048]{1,0:T(8,128)(2,1)} %param.21) | copy-start | bytes 393220
  97.5 25.1 %copy-start.7 = (f32[2048]{0:T(1024)S(1)}, f32[2048]{0:T(1024)}, u32[]{:S(2)}) copy-start(f32[2048]{0:T(1024)} %param.22) | copy-start | bytes 24580
  101.5 112.8 %reduce-scatter.5.cloned.1.call-start = ((), (), s32[]{:S(2)}) async-start(), calls=%async_computation.5 | async-start | bytes 2621440 | tf_op jit(solution)/shard_map/reduce_scatter | solution.py:140
  143.5 8.6 %collective-permute-start.3 = (bf16[4,32,2048]{2,1,0:T(8,128)(2,1)S(1)}, bf16[4,32,2048]{2,1,0:T(8,128)(2,1)S(1)}, u32[]{:S(2)}, u32[]{:S(2)}) collective-permute-start(bf16[4,32,2048]{2,1,0:T(8,128)(2,1)S(1)} %all_to_all.10), channel_id=1, source_target_pairs={{0,1},{1,2},{2,3},{3,0},{4,5},{5,6},{6,7},{7,4},{8,9},{9,10},{10,1... | collective-permute-start | bytes 1572872 | tf_op jit(solution)/shard_map/ppermute | solution.py:126
  152.9 8.7 %collective-permute-start.4 = (bf16[4,32,2048]{2,1,0:T(8,128)(2,1)S(1)}, bf16[4,32,2048]{2,1,0:T(8,128)(2,1)}, u32[]{:S(2)}, u32[]{:S(2)}) collective-permute-start(bf16[4,32,2048]{2,1,0:T(8,128)(2,1)S(1)} %collective-permute-done.3), channel_id=1, source_target_pairs={{0,1},{1,2},{2,3},{3,0},{4,5},{5,6},{6,7},{7,4},{8,9},{9,10},{10,1... | collective-permute-start | bytes 1572872 | tf_op jit(solution)/shard_map/ppermute | solution.py:126
  161.6 8.9 %collective-permute-start.5 = (bf16[4,32,2048]{2,1,0:T(8,128)(2,1)}, bf16[4,32,2048]{2,1,0:T(8,128)(2,1)}, u32[]{:S(2)}, u32[]{:S(2)}) collective-permute-start(bf16[4,32,2048]{2,1,0:T(8,128)(2,1)} %collective-permute-done.4), channel_id=1, source_target_pairs={{0,1},{1,2},{2,3},{3,0},{4,5},{5,6},{6,7},{7,4},{8,9},{9,10},{10,1... | collective-permute-start | bytes 1572872 | tf_op jit(solution)/shard_map/ppermute | solution.py:126
  161.6 12.2 %copy-start.2 = (bf16[4,32,2048]{2,1,0:T(8,128)(2,1)S(1)}, bf16[4,32,2048]{2,1,0:T(8,128)(2,1)}, u32[]{:S(2)}) copy-start(bf16[4,32,2048]{2,1,0:T(8,128)(2,1)} %copy-done.1) | copy-start | bytes 1572868
  161.6 14.4 %copy-start.4 = (bf16[4,32,2048]{2,1,0:T(8,128)(2,1)S(1)}, bf16[4,32,2048]{2,1,0:T(8,128)(2,1)}, u32[]{:S(2)}) copy-start(bf16[4,32,2048]{2,1,0:T(8,128)(2,1)} %copy-done.3) | copy-start | bytes 1572868
  176.0 1.9 copy-start.10
  184.9 48.5 %copy-start.9 = (f32[32,2]{0,1:T(2,128)S(1)}, f32[32,2]{0,1:T(2,128)}, u32[]{:S(2)}) copy-start(f32[32,2]{0,1:T(2,128)} %param.24) | copy-start | bytes 772
  184.9 49.8 %copy-start.6 = (bf16[32,2048]{1,0:T(8,128)(2,1)S(1)}, bf16[32,2048]{1,0:T(8,128)(2,1)}, u32[]{:S(2)}) copy-start(bf16[32,2048]{1,0:T(8,128)(2,1)} %reduce-scatter.3.cloned.1.call-done) | copy-start | bytes 393220
  214.4 19.0 %all-to-all-start.1 = ((bf16[4,32,2048]{2,1,0:T(8,128)(2,1)}), bf16[4,32,2048]{2,1,0:T(8,128)(2,1)}, u32[]{:S(2)}, u32[]{:S(2)}) async-start(bf16[4,32,2048]{2,1,0:T(8,128)(2,1)} %bitcast.78), calls=%async_computation.3 | async-start | bytes 1048576 | tf_op jit(solution)/shard_map/all_to_all | solution.py:147
  (3 other events, 3.5 us)
Sparse Core Ops, SparseCore 0:
  101.7 19.8 reduce-scatter.2
  185.0 29.3 reduce-scatter.4
